TPU v7x, 512 devices: a whole 4x4x16 slice. The times are simulated.
512 devices in a mesh: sp: 16 (over z), fs: 4 (over y), tp: 8 (over x, core).
Axes of the slice: x: 4, y: 4, z: 16, core: 2. Of those that a mesh axis runs over, the one named last changes fastest.
Arguments:
- tokens: bfloat16 [8192, 2048], P(('fs', 'sp'), 'tp'), parts along dimension 0, may hold values from -6 to 6
- norm_gain: float32 [2048], replicated, may hold values from 0.1 to 1.9
- w_recept: bfloat16 [2048, 1024], P('sp', 'tp'), may hold values from -0.125 to 0.125
- w_key_a: bfloat16 [2048, 1024], P('sp', 'tp'), may hold values from -0.125 to 0.125
- w_value_a: bfloat16 [2048, 1024], P('sp', 'tp'), may hold values from -0.125 to 0.125
- w_gate_a: bfloat16 [2048, 1024], P('sp', 'tp'), may hold values from -0.125 to 0.125
- decay_down_weight: bfloat16 [2048, 64], replicated, may hold values from -0.125 to 0.125
- decay_up_weight: bfloat16 [64, 1024], P(None, 'tp'), may hold values from -0.75 to 0.75
- rate_down_weight: bfloat16 [2048, 64], replicated, may hold values from -0.125 to 0.125
- rate_up_weight: bfloat16 [64, 1024], P(None, 'tp'), may hold values from -0.75 to 0.75
- decay_base: float32 [1024], P('tp'), may hold values from -12 to -2.5
- rate_base: float32 [1024], P('tp'), may hold values from -12 to 1
- rate_shift: float32 [8192, 16], P(('fs', 'sp'), 'tp'), parts along dimension 0, may hold values from 0 to 1.39
- jolts: float32 [8192, 16], P(('fs', 'sp'), 'tp'), parts along dimension 0, may hold values from 0 to 0.69
- group_gain: float32 [1024], P('tp'), may hold values from 0.1 to 1.9
- w_query_b: bfloat16 [2048, 1024], P('sp', 'tp'), may hold values from -0.125 to 0.125
- w_key_b: bfloat16 [2048, 1024], P('sp', 'tp'), may hold values from -0.125 to 0.125
- w_value_b: bfloat16 [2048, 1024], P('sp', 'tp'), may hold values from -0.125 to 0.125
- w_gate_b: bfloat16 [2048, 1024], P('sp', 'tp'), may hold values from -0.125 to 0.125
- score_offset: float32 [8], P('tp'), may hold values from -12 to -1
- w_out_a: bfloat16 [1024, 2048], P('tp'), may hold values from -0.125 to 0.125
- w_out_b: bfloat16 [1024, 2048], P('tp'), may hold values from -0.125 to 0.125
Outputs:
- mixed: bfloat16 [8192, 2048], P(('fs', 'sp', 'tp')), parts along dimension 0
- row_log: float32 [8192, 8], P(('fs', 'sp'), 'tp'), parts along dimension 0
There are 4 independent parts, one for each index of `fs`. A program takes and returns all parts, laid end to end along the dimension named above; an argument that names none is the same for every part. Nothing has to cross between parts.
All inputs are finite; a program needn't handle non-finite values.
Results may differ from a plain program's by a relative error of at most 0.02.
Values may be sent and summed in bfloat16 or wider, within the bound.
No kernel may reach another device: no remote copies, remote signals or barrier semaphores. Data moves between devices by JAX's collectives and lax.ppermute only.
A program may use at most 64 MiB of HBM per device.

v0:
```python
import jax
import jax.numpy as jnp
from jax import lax
from jax.sharding import PartitionSpec as P

HEAD_A = 64
HEAD_B = 128


def copy_for_each(value, axis):
    devices = lax.axis_size(axis)
    return lax.all_to_all(
        jnp.broadcast_to(value[None], (devices, *value.shape)), axis, 0, 0, tiled=True
    )


def laid_out(pieces, dim):
    pieces = jnp.moveaxis(pieces, 0, dim)
    shape = pieces.shape
    return pieces.reshape(*shape[:dim], shape[dim] * shape[dim + 1], *shape[dim + 2 :])


def collect(value, axis, dim):
    pieces = copy_for_each(value, axis)
    return laid_out(pieces, dim)


def in_one_piece(arrays, axis, dim, along):
    ends, at = ([], 0)
    for a in arrays[:-1]:
        at += a.shape[along]
        ends.append(at)
    both = jnp.concatenate(arrays, axis=along)
    return tuple(jnp.split(lax.all_gather(both, axis, axis=dim, tiled=True), ends, axis=along))


def gathered_once(value, axis):
    leaves = jax.tree.leaves(value)
    order = sorted(range(len(leaves)), key=lambda k: -leaves[k].size)
    width = (1, *leaves[order[0]].shape)[-1]
    lines = [
        jnp.pad(leaves[k].reshape(-1), (0, -leaves[k].size % width)).reshape(-1, width)
        for k in order
    ]
    both, at, found = (copy_for_each(jnp.concatenate(lines), axis), 0, {})
    for k, line in zip(order, lines):
        piece = both[:, at : at + len(line)].reshape(len(both), -1)
        found[k] = piece[:, : leaves[k].size].reshape(-1, *leaves[k].shape)
        at += len(line)
    numbers = iter(range(len(leaves)))
    return jax.tree.map(lambda _: found[next(numbers)], value)


def combined_pairwise(pieces, combine):
    while len(jax.tree.leaves(pieces)[0]) > 1:
        pieces = jax.vmap(combine)(
            *(jax.tree.map(lambda part: part[side::2], pieces) for side in (0, 1))
        )
    return jax.tree.map(lambda part: part[0], pieces)


def prefix_2(value, axis, combine, identity):
    devices, index = (lax.axis_size(axis), lax.axis_index(axis))
    passed = jnp.arange(devices) < index

    def kept(part, zero, own):
        part = jnp.where(
            passed.reshape(-1, *(1 for _ in own.shape)),
            part.astype(own.dtype),
            jnp.asarray(zero, own.dtype),
        )
        return part

    pieces = gathered_once(
        jax.tree.map(lambda part, kind: part.astype(kind), value, (jnp.bfloat16, jnp.bfloat16)),
        axis,
    )
    return combined_pairwise(jax.tree.map(kept, pieces, identity, value), combine)


def cut_along(value, dim, devices):
    before, after = (value.shape[:dim], value.shape[dim + 1 :])
    return jnp.moveaxis(value.reshape(*before, devices, -1, *after), dim, 0)


def sent_and_summed(value, axis, dim):
    devices = lax.axis_size(axis)
    pieces = lax.all_to_all(cut_along(value, dim, devices), axis, 0, 0, tiled=True)
    return jnp.sum(pieces.astype(jnp.float32), axis=0)


def combine_states(earlier, follower):
    joined = jnp.einsum("hij,hjk->hik", earlier[0], follower[0])
    carried = jnp.einsum("hij,hjk->hik", earlier[1], follower[0]) + follower[1]
    return (joined, carried)


def block_pass(stacked, pieces):
    recept_c, logs_step, keys_c, values_c, unit_c, mixing_c = pieces
    block_len = recept_c.shape[0]
    totals = jnp.cumsum(logs_step, axis=0)
    preceding = jnp.concatenate([jnp.zeros_like(totals[:1]), totals[:-1]], axis=0)
    steering = unit_c * mixing_c
    places_here = jnp.arange(block_len, dtype=jnp.int32)
    below_diag = (places_here[:, None] > places_here[None, :])[:, :, None, None]
    fading = jnp.where(
        below_diag, jnp.exp(jnp.where(below_diag, preceding[:, None] - totals[None, :], 0.0)), 0.0
    )
    unit_fade = fading * unit_c[:, None]
    weigh_keys = jnp.einsum("tjhc,jhc->htj", unit_fade, keys_c)
    weigh_steer = jnp.einsum("tjhc,jhc->htj", unit_fade, steering)
    read_fade = fading * (recept_c * jnp.exp(logs_step))[:, None]
    diagonal = jnp.eye(block_len, dtype=jnp.float32)
    read_keys = (
        jnp.einsum("tjhc,jhc->htj", read_fade, keys_c)
        + diagonal * jnp.sum(recept_c * keys_c, axis=2).T[:, :, None]
    )
    read_steer = (
        jnp.einsum("tjhc,jhc->htj", read_fade, steering)
        + diagonal * jnp.sum(recept_c * steering, axis=2).T[:, :, None]
    )
    values_wide = jnp.concatenate([jnp.zeros_like(values_c), values_c], axis=2)
    entering = jnp.einsum("thc,hrc->htr", unit_c * jnp.exp(preceding), stacked)
    entering = entering + jnp.einsum("htj,jhr->htr", weigh_keys, values_wide)
    removal = jax.scipy.linalg.solve_triangular(
        weigh_steer + diagonal, entering, lower=True, unit_diagonal=True
    )
    readout = jnp.einsum("thc,hrc->htr", recept_c * jnp.exp(totals), stacked)
    readout = readout + jnp.einsum("htj,jhr->htr", read_keys, values_wide)
    readout = readout - jnp.einsum("htj,hjr->htr", read_steer, removal)
    tail_fade = jnp.exp(totals[-1][None] - totals)
    closing = stacked * jnp.exp(totals[-1])[:, None, :]
    closing = closing + jnp.einsum("jhr,jhc->hrc", values_wide, keys_c * tail_fade)
    closing = closing - jnp.einsum("hjr,jhc->hrc", removal, steering * tail_fade)
    return (closing, jnp.transpose(readout, (1, 0, 2)))


def local(
    tokens,
    norm_gain,
    w_recept,
    w_key_a,
    w_value_a,
    w_gate_a,
    decay_down_weight,
    decay_up_weight,
    rate_down_weight,
    rate_up_weight,
    decay_base,
    rate_base,
    rate_shift,
    jolts,
    group_gain,
    w_query_b,
    w_key_b,
    w_value_b,
    w_gate_b,
    score_offset,
    w_out_a,
    w_out_b,
):
    gathered = collect(tokens, "tp", 1)
    floats = gathered.astype(jnp.float32)
    normed = (
        floats * lax.rsqrt(jnp.mean(floats * floats, axis=1, keepdims=True) + 1e-06) * norm_gain
    ).astype(jnp.bfloat16)
    row_count = normed.shape[0]
    matrices = (w_recept, w_key_a, w_value_a, w_gate_a, w_query_b, w_key_b, w_value_b, w_gate_b)
    portions = in_one_piece(
        (
            matrices[0],
            matrices[1],
            matrices[2],
            matrices[3],
            matrices[4],
            matrices[5],
            matrices[6],
            matrices[7],
        ),
        "sp",
        0,
        1,
    )
    projected = tuple(
        (jnp.dot(normed, portion, preferred_element_type=jnp.float32) for portion in portions)
    )
    recept, keys_a, values_a, gate_a, query_b, keys_b, values_b, gate_b = [
        summed.astype(jnp.bfloat16) for summed in projected
    ]
    heads_a = recept.shape[1] // HEAD_A
    decay_low = jnp.tanh(
        jnp.dot(normed, decay_down_weight, preferred_element_type=jnp.float32)
    ).astype(jnp.bfloat16)
    rate_low = jnp.dot(normed, rate_down_weight, preferred_element_type=jnp.float32).astype(
        jnp.bfloat16
    )
    preact = (
        decay_base
        + jnp.dot(decay_low, decay_up_weight, preferred_element_type=jnp.float32)
        + jnp.repeat(rate_shift, HEAD_A, axis=1)
    )
    log_decay = -jnp.exp(-jax.nn.softplus(-preact) - 0.5) - jnp.repeat(jolts, HEAD_A, axis=1)
    mixing = jax.nn.sigmoid(
        rate_base + jnp.dot(rate_low, rate_up_weight, preferred_element_type=jnp.float32)
    )

    def split_heads(matrix):
        return matrix.astype(jnp.float32).reshape(row_count, heads_a, HEAD_A)

    keys_heads = split_heads(keys_a)
    unit_keys = keys_heads * lax.rsqrt(
        jnp.sum(keys_heads * keys_heads, axis=2, keepdims=True) + 1e-06
    )
    block_len = min(32, row_count)
    block_count = row_count // block_len

    def to_blocks(matrix):
        return matrix.reshape(block_count, block_len, heads_a, HEAD_A)

    inputs = tuple(
        (
            to_blocks(matrix)
            for matrix in (
                split_heads(recept),
                log_decay.reshape(row_count, heads_a, HEAD_A),
                keys_heads,
                split_heads(values_a),
                unit_keys,
                mixing.reshape(row_count, heads_a, HEAD_A),
            )
        )
    )
    identity = jnp.broadcast_to(jnp.eye(HEAD_A, dtype=jnp.float32), (heads_a, HEAD_A, HEAD_A))
    zeros_state = jnp.zeros((heads_a, HEAD_A, HEAD_A), jnp.float32)
    closing, readout = lax.scan(
        block_pass, jnp.concatenate([identity, zeros_state], axis=1), inputs
    )
    readout = readout.reshape(row_count, heads_a, 2 * HEAD_A)
    prefix = prefix_2(
        (closing[:, :HEAD_A], closing[:, HEAD_A:]), "sp", combine_states, (identity, zeros_state)
    )
    outputs_a = readout[:, :, HEAD_A:] + jnp.einsum(
        "hvk,thk->thv", prefix[1], readout[:, :, :HEAD_A]
    )
    centered = outputs_a - jnp.mean(outputs_a, axis=2, keepdims=True)
    normal_a = centered * lax.rsqrt(jnp.mean(centered * centered, axis=2, keepdims=True) + 0.00064)
    mixed_a = (
        normal_a.reshape(row_count, -1) * group_gain * jax.nn.silu(gate_a.astype(jnp.float32))
    ).astype(jnp.bfloat16)
    heads_b = query_b.shape[1] // HEAD_B
    own_index = lax.axis_index("sp")
    places = jnp.arange(row_count, dtype=jnp.int32)
    query_place = own_index * row_count + places
    query_heads = query_b.reshape(row_count, heads_b, HEAD_B)
    factor = HEAD_B ** (-0.5)
    paired = jnp.stack(
        [keys_b.reshape(row_count, heads_b, HEAD_B), values_b.reshape(row_count, heads_b, HEAD_B)]
    )

    def attend(running, paired_piece, source):
        attended, weight_sum, survive = running
        scores = (
            jnp.einsum(
                "qhd,khd->hqk", query_heads, paired_piece[0], preferred_element_type=jnp.float32
            )
            * factor
            + score_offset[:, None, None]
        )
        causal = (source * row_count + places)[None, None, :] < query_place[None, :, None]
        keep_log = jnp.where(causal, jax.nn.log_sigmoid(-scores), 0.0)
        later_sum = (
            jnp.flip(jnp.cumsum(jnp.flip(keep_log, 2), axis=2), 2) - keep_log + survive[:, :, None]
        )
        weights = jnp.where(causal, jnp.exp(jax.nn.log_sigmoid(scores) + later_sum), 0.0)
        attended = attended + jnp.einsum(
            "hqk,khd->qhd",
            weights.astype(jnp.bfloat16),
            paired_piece[1],
            preferred_element_type=jnp.float32,
        )
        return (
            attended,
            weight_sum + jnp.sum(weights, axis=2),
            survive + jnp.sum(keep_log, axis=2),
        )

    empty_b = (
        jnp.zeros((row_count, heads_b, HEAD_B), jnp.float32),
        jnp.zeros((heads_b, row_count), jnp.float32),
        jnp.zeros((heads_b, row_count), jnp.float32),
    )
    running = attend(empty_b, paired, own_index)
    all_pairs = lax.all_gather(paired[None], "sp", axis=0, tiled=True)

    def visit_piece(rounds, holding):
        source = own_index - rounds
        chosen = lax.dynamic_index_in_dim(all_pairs, jnp.maximum(source, 0), 0, False)
        return lax.cond(
            source >= 0, lambda kept: attend(kept, chosen, source), lambda kept: kept, holding
        )

    running = lax.fori_loop(1, lax.axis_size("sp"), visit_piece, running)
    mixed_b = (running[0].reshape(row_count, -1) * jax.nn.silu(gate_b.astype(jnp.float32))).astype(
        jnp.bfloat16
    )
    row_log = jnp.log(jnp.maximum(running[1].T, 0.01))
    mixed = sent_and_summed(
        (
            jnp.dot(mixed_a, w_out_a, preferred_element_type=jnp.float32)
            + jnp.dot(mixed_b, w_out_b, preferred_element_type=jnp.float32)
        ).astype(jnp.bfloat16),
        "tp",
        0,
    )
    return (mixed.astype(jnp.bfloat16), row_log)


def solution(mesh):
    in_specs = (
        P(("fs", "sp"), "tp"),
        P(),
        P("sp", "tp"),
        P("sp", "tp"),
        P("sp", "tp"),
        P("sp", "tp"),
        P(),
        P(None, "tp"),
        P(),
        P(None, "tp"),
        P("tp"),
        P("tp"),
        P(("fs", "sp"), "tp"),
        P(("fs", "sp"), "tp"),
        P("tp"),
        P("sp", "tp"),
        P("sp", "tp"),
        P("sp", "tp"),
        P("sp", "tp"),
        P("tp"),
        P("tp", None),
        P("tp", None),
    )
    out_specs = (P(("fs", "sp", "tp"), None), P(("fs", "sp"), "tp"))
    return jax.shard_map(local, mesh=mesh, in_specs=in_specs, out_specs=out_specs, check_vma=False)
```

profile of v0, /device:TPU:504, one launch (start us, length us, event | category | flops | bytes accessed | tf_op | source)
XLA Modules:
  0.0 244.6 jit_solution(12712214649210133443)
XLA Ops:
  16.1 4.3 %all-to-all-start = ((bf16[8,128,256]{1,2,0:T(8,128)(2,1)}), bf16[8,128,256]{1,2,0:T(8,128)(2,1)S(1)}, u32[]{:S(2)}, u32[]{:S(2)}) async-start(bf16[8,128,256]{1,2,0:T(8,128)(2,1)} %broadcast_in_dim.74), calls=%async_computation | async-start | bytes 1048576 | tf_op jit(solution)/shard_map/all_to_all | solution.py:12
  22.1 8.6 %all-to-all-done = bf16[8,128,256]{1,2,0:T(8,128)(2,1)S(1)} async-done(((bf16[8,128,256]{1,2,0:T(8,128)(2,1)}), bf16[8,128,256]{1,2,0:T(8,128)(2,1)S(1)}, u32[]{:S(2)}, u32[]{:S(2)}) %all-to-all-start) | async-done | bytes 524320 | tf_op jit(solution)/shard_map/all_to_all | solution.py:12
  33.3 56.6 %all-gather.4.cloned.1.call-done = bf16[2048,1024]{1,0:T(8,128)(2,1)} async-done(((bf16[128,1024]{1,0:T(8,128)(2,1)}), bf16[2048,1024]{1,0:T(8,128)(2,1)}) %all-gather.4.cloned.1.call-update) | async-done | bytes 4194320 | tf_op jit(solution)/shard_map/all_gather | solution.py:34
  98.3 48.1 %while.30 = (s32[]{:T(128)}, f32[2,128,64]{1,2,0:T(8,128)S(1)}, f32[4,32,2,128]{3,1,0,2:T(8,128)S(1)}, f32[4,32,2,64]{3,2,1,0:T(2,128)S(1)}, bf16[4,32,2,64]{3,2...) while((s32[]{:T(128)}, f32[2,128,64]{1,2,0:T(8,128)S(1)}, ...), condition=%wide.region_6.7_spmd, body=%wide.region_2.6_spmd.sunk | while | flops 11161506 | bytes 3108997 | solution.py:235
  98.5 1.8 fusion.243
  102.6 4.9 %custom-call.8 = f32[2,1,32,32]{2,3,1,0:T(8,128)S(1)} custom-call(f32[2,1,32,32]{3,2,1,0:T(8,128)S(1)} %fusion.247), custom_call_target="InvertDiagBlocksLowerTriangular" | custom-call | tf_op jit(solution)/shard_map/while/body/eval_jaxpr/jit(_solve_triangular)/vmap()/triangular_solve | solution.py:125
  110.6 1.8 fusion.243
  114.6 4.9 %custom-call.8 = f32[2,1,32,32]{2,3,1,0:T(8,128)S(1)} custom-call(f32[2,1,32,32]{3,2,1,0:T(8,128)S(1)} %fusion.247), custom_call_target="InvertDiagBlocksLowerTriangular" | custom-call | tf_op jit(solution)/shard_map/while/body/eval_jaxpr/jit(_solve_triangular)/vmap()/triangular_solve | solution.py:125
  122.6 1.8 fusion.243
  126.6 4.9 %custom-call.8 = f32[2,1,32,32]{2,3,1,0:T(8,128)S(1)} custom-call(f32[2,1,32,32]{3,2,1,0:T(8,128)S(1)} %fusion.247), custom_call_target="InvertDiagBlocksLowerTriangular" | custom-call | tf_op jit(solution)/shard_map/while/body/eval_jaxpr/jit(_solve_triangular)/vmap()/triangular_solve | solution.py:125
  134.6 1.8 fusion.243
  138.6 4.9 %custom-call.8 = f32[2,1,32,32]{2,3,1,0:T(8,128)S(1)} custom-call(f32[2,1,32,32]{3,2,1,0:T(8,128)S(1)} %fusion.247), custom_call_target="InvertDiagBlocksLowerTriangular" | custom-call | tf_op jit(solution)/shard_map/while/body/eval_jaxpr/jit(_solve_triangular)/vmap()/triangular_solve | solution.py:125
  147.6 7.8 %all-to-all-start.1 = ((bf16[16,256,64]{1,2,0:T(8,128)(2,1)}), bf16[16,256,64]{1,2,0:T(8,128)(2,1)S(1)}, u32[]{:S(2)}, u32[]{:S(2)}) async-start(bf16[16,256,64]{1,2,0:T(8,128)(2,1)} %broadcast_in_dim.107), calls=%async_computation.1 | async-start | bytes 1048576 | tf_op jit(solution)/shard_map/all_to_all | solution.py:12
  158.9 5.9 %all-gather.6.cloned.1.call-done = bf16[32,128,1,128]{3,1,2,0:T(8,128)(2,1)} async-done(((bf16[2,128,1,128]{3,1,2,0:T(8,128)(2,1)}), bf16[32,128,1,128]{3,1,2,0:T(8,128)(2,1)}) %all-gather.6.cloned.1.call-update) | async-done | bytes 1048592 | tf_op jit(solution)/shard_map/all_gather | solution.py:293
  164.8 45.0 %while.31 = (s32[]{:T(128)}, f32[128,1,128]{0,2,1:T(8,128)S(1)}, f32[1,128]{1,0:T(1,128)S(1)}, f32[1,128]{1,0:T(1,128)S(1)}, s32[]{:T(128)}, /*index=5*/bf16[16,...) while((s32[]{:T(128)}, f32[128,1,128]{0,2,1:T(8,128)S(1)}, ...), condition=%wide.region_18.19_spmd.clone, body=%wide.region_12.18_spmd.clone.sunk | while | flops 11075848 | bytes 960331 | solution.py:302
  164.8 2.9 %conditional.3 = ((f32[128,1,128]{0,2,1:T(8,128)S(1)}, f32[1,128]{1,0:T(1,128)S(1)}, f32[1,128]{1,0:T(1,128)S(1)})) conditional(s32[]{:T(128)} %convert_element_type.212, (f32[128,1,128]{0,2,1:T(8,128)S(1)}, f32[1,128]{1,0:T(1,128)S(1)}, f32[1,128]{1,0:T(1,128)S(1)}) %tuple.100, (s32[]{:T(128)}, bf16[16,2,128,1,128]{4,2,3,1,0:T(8,128)(2,1)}, ...), branch_computations={%region_13.13_spmd, %region_14.17_spmd} | conditional | flops 11075843 | bytes 959580 | solution.py:298
  167.7 3.0 %conditional.3 = ((f32[128,1,128]{0,2,1:T(8,128)S(1)}, f32[1,128]{1,0:T(1,128)S(1)}, f32[1,128]{1,0:T(1,128)S(1)})) conditional(s32[]{:T(128)} %convert_element_type.212, (f32[128,1,128]{0,2,1:T(8,128)S(1)}, f32[1,128]{1,0:T(1,128)S(1)}, f32[1,128]{1,0:T(1,128)S(1)}) %tuple.100, (s32[]{:T(128)}, bf16[16,2,128,1,128]{4,2,3,1,0:T(8,128)(2,1)}, ...), branch_computations={%region_13.13_spmd, %region_14.17_spmd} | conditional | flops 11075843 | bytes 959580 | solution.py:298
  167.8 1.6 fusion.69
  170.7 3.0 %conditional.3 = ((f32[128,1,128]{0,2,1:T(8,128)S(1)}, f32[1,128]{1,0:T(1,128)S(1)}, f32[1,128]{1,0:T(1,128)S(1)})) conditional(s32[]{:T(128)} %convert_element_type.212, (f32[128,1,128]{0,2,1:T(8,128)S(1)}, f32[1,128]{1,0:T(1,128)S(1)}, f32[1,128]{1,0:T(1,128)S(1)}) %tuple.100, (s32[]{:T(128)}, bf16[16,2,128,1,128]{4,2,3,1,0:T(8,128)(2,1)}, ...), branch_computations={%region_13.13_spmd, %region_14.17_spmd} | conditional | flops 11075843 | bytes 959580 | solution.py:298
  170.8 1.6 fusion.69
  173.7 3.0 %conditional.3 = ((f32[128,1,128]{0,2,1:T(8,128)S(1)}, f32[1,128]{1,0:T(1,128)S(1)}, f32[1,128]{1,0:T(1,128)S(1)})) conditional(s32[]{:T(128)} %convert_element_type.212, (f32[128,1,128]{0,2,1:T(8,128)S(1)}, f32[1,128]{1,0:T(1,128)S(1)}, f32[1,128]{1,0:T(1,128)S(1)}) %tuple.100, (s32[]{:T(128)}, bf16[16,2,128,1,128]{4,2,3,1,0:T(8,128)(2,1)}, ...), branch_computations={%region_13.13_spmd, %region_14.17_spmd} | conditional | flops 11075843 | bytes 959580 | solution.py:298
  173.8 1.6 fusion.69
  176.7 3.0 %conditional.3 = ((f32[128,1,128]{0,2,1:T(8,128)S(1)}, f32[1,128]{1,0:T(1,128)S(1)}, f32[1,128]{1,0:T(1,128)S(1)})) conditional(s32[]{:T(128)} %convert_element_type.212, (f32[128,1,128]{0,2,1:T(8,128)S(1)}, f32[1,128]{1,0:T(1,128)S(1)}, f32[1,128]{1,0:T(1,128)S(1)}) %tuple.100, (s32[]{:T(128)}, bf16[16,2,128,1,128]{4,2,3,1,0:T(8,128)(2,1)}, ...), branch_computations={%region_13.13_spmd, %region_14.17_spmd} | conditional | flops 11075843 | bytes 959580 | solution.py:298
  176.8 1.6 fusion.69
  179.7 3.0 %conditional.3 = ((f32[128,1,128]{0,2,1:T(8,128)S(1)}, f32[1,128]{1,0:T(1,128)S(1)}, f32[1,128]{1,0:T(1,128)S(1)})) conditional(s32[]{:T(128)} %convert_element_type.212, (f32[128,1,128]{0,2,1:T(8,128)S(1)}, f32[1,128]{1,0:T(1,128)S(1)}, f32[1,128]{1,0:T(1,128)S(1)}) %tuple.100, (s32[]{:T(128)}, bf16[16,2,128,1,128]{4,2,3,1,0:T(8,128)(2,1)}, ...), branch_computations={%region_13.13_spmd, %region_14.17_spmd} | conditional | flops 11075843 | bytes 959580 | solution.py:298
  179.8 1.6 fusion.69
  182.7 3.0 %conditional.3 = ((f32[128,1,128]{0,2,1:T(8,128)S(1)}, f32[1,128]{1,0:T(1,128)S(1)}, f32[1,128]{1,0:T(1,128)S(1)})) conditional(s32[]{:T(128)} %convert_element_type.212, (f32[128,1,128]{0,2,1:T(8,128)S(1)}, f32[1,128]{1,0:T(1,128)S(1)}, f32[1,128]{1,0:T(1,128)S(1)}) %tuple.100, (s32[]{:T(128)}, bf16[16,2,128,1,128]{4,2,3,1,0:T(8,128)(2,1)}, ...), branch_computations={%region_13.13_spmd, %region_14.17_spmd} | conditional | flops 11075843 | bytes 959580 | solution.py:298
  182.8 1.6 fusion.69
  185.7 3.0 %conditional.3 = ((f32[128,1,128]{0,2,1:T(8,128)S(1)}, f32[1,128]{1,0:T(1,128)S(1)}, f32[1,128]{1,0:T(1,128)S(1)})) conditional(s32[]{:T(128)} %convert_element_type.212, (f32[128,1,128]{0,2,1:T(8,128)S(1)}, f32[1,128]{1,0:T(1,128)S(1)}, f32[1,128]{1,0:T(1,128)S(1)}) %tuple.100, (s32[]{:T(128)}, bf16[16,2,128,1,128]{4,2,3,1,0:T(8,128)(2,1)}, ...), branch_computations={%region_13.13_spmd, %region_14.17_spmd} | conditional | flops 11075843 | bytes 959580 | solution.py:298
  185.8 1.6 fusion.69
  188.7 3.0 %conditional.3 = ((f32[128,1,128]{0,2,1:T(8,128)S(1)}, f32[1,128]{1,0:T(1,128)S(1)}, f32[1,128]{1,0:T(1,128)S(1)})) conditional(s32[]{:T(128)} %convert_element_type.212, (f32[128,1,128]{0,2,1:T(8,128)S(1)}, f32[1,128]{1,0:T(1,128)S(1)}, f32[1,128]{1,0:T(1,128)S(1)}) %tuple.100, (s32[]{:T(128)}, bf16[16,2,128,1,128]{4,2,3,1,0:T(8,128)(2,1)}, ...), branch_computations={%region_13.13_spmd, %region_14.17_spmd} | conditional | flops 11075843 | bytes 959580 | solution.py:298
  188.8 1.6 fusion.69
  191.8 3.0 %conditional.3 = ((f32[128,1,128]{0,2,1:T(8,128)S(1)}, f32[1,128]{1,0:T(1,128)S(1)}, f32[1,128]{1,0:T(1,128)S(1)})) conditional(s32[]{:T(128)} %convert_element_type.212, (f32[128,1,128]{0,2,1:T(8,128)S(1)}, f32[1,128]{1,0:T(1,128)S(1)}, f32[1,128]{1,0:T(1,128)S(1)}) %tuple.100, (s32[]{:T(128)}, bf16[16,2,128,1,128]{4,2,3,1,0:T(8,128)(2,1)}, ...), branch_computations={%region_13.13_spmd, %region_14.17_spmd} | conditional | flops 11075843 | bytes 959580 | solution.py:298
  191.8 1.6 fusion.69
  194.8 3.0 %conditional.3 = ((f32[128,1,128]{0,2,1:T(8,128)S(1)}, f32[1,128]{1,0:T(1,128)S(1)}, f32[1,128]{1,0:T(1,128)S(1)})) conditional(s32[]{:T(128)} %convert_element_type.212, (f32[128,1,128]{0,2,1:T(8,128)S(1)}, f32[1,128]{1,0:T(1,128)S(1)}, f32[1,128]{1,0:T(1,128)S(1)}) %tuple.100, (s32[]{:T(128)}, bf16[16,2,128,1,128]{4,2,3,1,0:T(8,128)(2,1)}, ...), branch_computations={%region_13.13_spmd, %region_14.17_spmd} | conditional | flops 11075843 | bytes 959580 | solution.py:298
  194.8 1.6 fusion.69
  197.8 3.0 %conditional.3 = ((f32[128,1,128]{0,2,1:T(8,128)S(1)}, f32[1,128]{1,0:T(1,128)S(1)}, f32[1,128]{1,0:T(1,128)S(1)})) conditional(s32[]{:T(128)} %convert_element_type.212, (f32[128,1,128]{0,2,1:T(8,128)S(1)}, f32[1,128]{1,0:T(1,128)S(1)}, f32[1,128]{1,0:T(1,128)S(1)}) %tuple.100, (s32[]{:T(128)}, bf16[16,2,128,1,128]{4,2,3,1,0:T(8,128)(2,1)}, ...), branch_computations={%region_13.13_spmd, %region_14.17_spmd} | conditional | flops 11075843 | bytes 959580 | solution.py:298
  197.8 1.6 fusion.69
  200.8 3.0 %conditional.3 = ((f32[128,1,128]{0,2,1:T(8,128)S(1)}, f32[1,128]{1,0:T(1,128)S(1)}, f32[1,128]{1,0:T(1,128)S(1)})) conditional(s32[]{:T(128)} %convert_element_type.212, (f32[128,1,128]{0,2,1:T(8,128)S(1)}, f32[1,128]{1,0:T(1,128)S(1)}, f32[1,128]{1,0:T(1,128)S(1)}) %tuple.100, (s32[]{:T(128)}, bf16[16,2,128,1,128]{4,2,3,1,0:T(8,128)(2,1)}, ...), branch_computations={%region_13.13_spmd, %region_14.17_spmd} | conditional | flops 11075843 | bytes 959580 | solution.py:298
  200.8 1.6 fusion.69
  203.8 3.0 %conditional.3 = ((f32[128,1,128]{0,2,1:T(8,128)S(1)}, f32[1,128]{1,0:T(1,128)S(1)}, f32[1,128]{1,0:T(1,128)S(1)})) conditional(s32[]{:T(128)} %convert_element_type.212, (f32[128,1,128]{0,2,1:T(8,128)S(1)}, f32[1,128]{1,0:T(1,128)S(1)}, f32[1,128]{1,0:T(1,128)S(1)}) %tuple.100, (s32[]{:T(128)}, bf16[16,2,128,1,128]{4,2,3,1,0:T(8,128)(2,1)}, ...), branch_computations={%region_13.13_spmd, %region_14.17_spmd} | conditional | flops 11075843 | bytes 959580 | solution.py:298
  203.8 1.6 fusion.69
  206.8 3.0 %conditional.3 = ((f32[128,1,128]{0,2,1:T(8,128)S(1)}, f32[1,128]{1,0:T(1,128)S(1)}, f32[1,128]{1,0:T(1,128)S(1)})) conditional(s32[]{:T(128)} %convert_element_type.212, (f32[128,1,128]{0,2,1:T(8,128)S(1)}, f32[1,128]{1,0:T(1,128)S(1)}, f32[1,128]{1,0:T(1,128)S(1)}) %tuple.100, (s32[]{:T(128)}, bf16[16,2,128,1,128]{4,2,3,1,0:T(8,128)(2,1)}, ...), branch_computations={%region_13.13_spmd, %region_14.17_spmd} | conditional | flops 11075843 | bytes 959580 | solution.py:298
  206.8 1.6 fusion.69
  212.4 1.6 fusion.133
  214.0 2.4 fusion.70
  216.5 10.2 %all-to-all-start.2 = ((bf16[8,16,2048]{2,1,0:T(8,128)(2,1)}), bf16[8,16,2048]{2,1,0:T(8,128)(2,1)S(1)}, u32[]{:S(2)}, u32[]{:S(2)}) async-start(bf16[8,16,2048]{2,1,0:T(8,128)(2,1)} %bitcast.66), calls=%async_computation.2 | async-start | bytes 1048576 | tf_op jit(solution)/shard_map/all_to_all | solution.py:88
  227.2 9.8 %all-to-all-done.2 = bf16[8,16,2048]{2,1,0:T(8,128)(2,1)S(1)} async-done(((bf16[8,16,2048]{2,1,0:T(8,128)(2,1)}), bf16[8,16,2048]{2,1,0:T(8,128)(2,1)S(1)}, u32[]{:S(2)}, u32[]{:S(2)}) %all-to-all-start.2) | async-done | bytes 524320 | tf_op jit(solution)/shard_map/all_to_all | solution.py:88
  (365 shorter events, 70.7 us)
Async XLA Ops:
  7.2 205.2 %copy-start = (bf16[128,2048]{1,0:T(8,128)(2,1)S(1)}, bf16[128,2048]{1,0:T(8,128)(2,1)}, u32[]{:S(2)}) copy-start(bf16[128,2048]{1,0:T(8,128)(2,1)} %param.48) | copy-start | bytes 1572868
  7.2 24.9 %copy-start.3 = (bf16[2048,64]{0,1:T(8,128)(2,1)S(1)}, bf16[2048,64]{0,1:T(8,128)(2,1)}, u32[]{:S(2)}) copy-start(bf16[2048,64]{0,1:T(8,128)(2,1)} %param.34) | copy-start | bytes 786436
  7.2 24.9 %copy-start.5 = (bf16[64,128]{1,0:T(8,128)(2,1)S(1)}, bf16[64,128]{1,0:T(8,128)(2,1)}, u32[]{:S(2)}) copy-start(bf16[64,128]{1,0:T(8,128)(2,1)} %param.35) | copy-start | bytes 49156
  7.2 24.9 %copy-start.7 = (f32[128]{0:T(128)S(1)}, f32[128]{0:T(128)}, u32[]{:S(2)}) copy-start(f32[128]{0:T(128)} %param.38) | copy-start | bytes 1540
  7.2 25.5 %copy-start.4 = (bf16[2048,64]{0,1:T(8,128)(2,1)S(1)}, bf16[2048,64]{0,1:T(8,128)(2,1)}, u32[]{:S(2)}) copy-start(bf16[2048,64]{0,1:T(8,128)(2,1)} %param.36) | copy-start | bytes 786436
  7.2 25.5 %copy-start.6 = (bf16[64,128]{1,0:T(8,128)(2,1)S(1)}, bf16[64,128]{1,0:T(8,128)(2,1)}, u32[]{:S(2)}) copy-start(bf16[64,128]{1,0:T(8,128)(2,1)} %param.37) | copy-start | bytes 49156
  7.2 25.5 %copy-start.8 = (f32[128]{0:T(128)S(1)}, f32[128]{0:T(128)}, u32[]{:S(2)}) copy-start(f32[128]{0:T(128)} %param.39) | copy-start | bytes 1540
  7.2 82.6 %all-gather.4.cloned.1.call-start = ((), (), s32[]{:S(2)}) async-start(), calls=%async_computation.3 | async-start | bytes 4456448 | tf_op jit(solution)/shard_map/all_gather | solution.py:34
  13.5 0.7 copy-start.2
  16.1 14.6 %all-to-all-start = ((bf16[8,128,256]{1,2,0:T(8,128)(2,1)}), bf16[8,128,256]{1,2,0:T(8,128)(2,1)S(1)}, u32[]{:S(2)}, u32[]{:S(2)}) async-start(bf16[8,128,256]{1,2,0:T(8,128)(2,1)} %broadcast_in_dim.74), calls=%async_computation | async-start | bytes 1048576 | tf_op jit(solution)/shard_map/all_to_all | solution.py:12
  20.4 144.4 %all-gather.6.cloned.1.call-start = ((), (), s32[]{:S(2)}) async-start(), calls=%async_computation.4 | async-start | bytes 1114112 | tf_op jit(solution)/shard_map/all_gather | solution.py:293
  147.6 62.3 %all-to-all-start.1 = ((bf16[16,256,64]{1,2,0:T(8,128)(2,1)}), bf16[16,256,64]{1,2,0:T(8,128)(2,1)S(1)}, u32[]{:S(2)}, u32[]{:S(2)}) async-start(bf16[16,256,64]{1,2,0:T(8,128)(2,1)} %broadcast_in_dim.107), calls=%async_computation.1 | async-start | bytes 1048576 | tf_op jit(solution)/shard_map/all_to_all | solution.py:12
  210.3 2.1 copy-start.9
  210.7 3.3 %copy-start.1 = (bf16[128,2048]{1,0:T(8,128)(2,1)S(1)}, bf16[128,2048]{1,0:T(8,128)(2,1)}, u32[]{:S(2)}) copy-start(bf16[128,2048]{1,0:T(8,128)(2,1)} %param.49) | copy-start | bytes 1572868
  216.5 20.6 %all-to-all-start.2 = ((bf16[8,16,2048]{2,1,0:T(8,128)(2,1)}), bf16[8,16,2048]{2,1,0:T(8,128)(2,1)S(1)}, u32[]{:S(2)}, u32[]{:S(2)}) async-start(bf16[8,16,2048]{2,1,0:T(8,128)(2,1)} %bitcast.66), calls=%async_computation.2 | async-start | bytes 1048576 | tf_op jit(solution)/shard_map/all_to_all | solution.py:88
Sparse Core Ops, SparseCore 0:
  14.4 75.4 all-gather.3
  93.4 71.2 all-gather.5
where the time goes:
time: 248 us; the launch traced here: 245 us
  waiting for transfers between devices  80.9 us (33%)
  matrix products  70.7 us (29%)
  other arithmetic  37.6 us (15%)
  starting transfers between devices  22.4 us (9%)
  local copies, waits for them, and re-layouts  16 us (6%)
  between operations  15.2 us (6%)
    all_gather x1, waiting for transfers between devices, in_one_piece(): lax.all_gather(both, axis, axis=dim, tiled=True)  56.6 us
    dot_general x16, matrix products, attend(): jnp.einsum('qhd,khd->hqk', query_heads, paired_piece[0], preferred_elemen...  24.5 us
    another operation x20, other arithmetic, block_pass(): jax.scipy.linalg.solve_triangular(weigh_steer + diagonal, entering, lower...  20.1 us
    dot_general x16, matrix products, attend(): jnp.einsum('hqk,khd->qhd', weights.astype(jnp.bfloat16), paired_piece[1],...  14.4 us
    all_to_all x2, starting transfers between devices, copy_for_each(): lax.all_to_all(jnp.broadcast_to(value[None], (devices, *value.shape)), ax...  12.1 us
    all_to_all x1, starting transfers between devices, sent_and_summed(): lax.all_to_all(cut_along(value, dim, devices), axis, 0, 0, tiled=True)  10.2 us
    all_to_all x1, waiting for transfers between devices, sent_and_summed(): lax.all_to_all(cut_along(value, dim, devices), axis, 0, 0, tiled=True)  9.8 us
    all_to_all x2, waiting for transfers between devices, copy_for_each(): lax.all_to_all(jnp.broadcast_to(value[None], (devices, *value.shape)), ax...  8.57 us
  transfers between devices with their start and end apart: 5, of which 4 were waited for; matrix products, arithmetic and copies ran while one was open for 44% of the time, Pallas kernels for 0%

commit v1 on v0

--- a/solution.py
+++ b/solution.py
@@ -1,3 +1,4 @@
+import functools
 import jax
 import jax.numpy as jnp
 from jax import lax
@@ -5,6 +6,22 @@
 
 HEAD_A = 64
 HEAD_B = 128
+
+
+def extend_waves(message, lane_axis):
+    o_now = jnp.concatenate(
+        lax.all_to_all(
+            jnp.stack(lax.axis_size(lane_axis) * [message]),
+            axis_name=lane_axis,
+            split_axis=0,
+            concat_axis=0,
+        ),
+        axis=0,
+    )
+    return o_now
+
+
+extend_the_sector = functools.partial(extend_waves, lane_axis="sp")
 
 
 def copy_for_each(value, axis):
@@ -290,7 +307,7 @@
         jnp.zeros((heads_b, row_count), jnp.float32),
     )
     running = attend(empty_b, paired, own_index)
-    all_pairs = lax.all_gather(paired[None], "sp", axis=0, tiled=True)
+    all_pairs = extend_the_sector(paired[None])
 
     def visit_piece(rounds, holding):
         source = own_index - rounds

time: 248 us -> 297 us (1.20)
  waiting for transfers between devices: 80.9 us -> 127 us
    all_to_all x0 -> x1, waiting for transfers between devices: none -> 37 us  [extend_waves(): lax.all_to_all(jnp.stack(lax.axis_size(lane_axis) * [message]), axis_name...]
    all_to_all x2, waiting for transfers between devices: 8.57 us -> 23.4 us  [copy_for_each(): lax.all_to_all(jnp.broadcast_to(value[None], (devices, *value.shape)), ax...]
    all_to_all x0 -> x1, starting transfers between devices: none -> 6.04 us  [extend_waves(): lax.all_to_all(jnp.stack(lax.axis_size(lane_axis) * [message]), axis_name...]
    all_gather x1 -> x0, waiting for transfers between devices: 5.9 us -> none  [local(): all_pairs = lax.all_gather(paired[None], 'sp', axis=0, tiled=True)]
    all_to_all x1, starting transfers between devices: 10.2 us -> 5.83 us  [sent_and_summed(): lax.all_to_all(cut_along(value, dim, devices), axis, 0, 0, tiled=True)]
  transfers between devices with their start and end apart: 5 -> 5, of which waited for: 4 -> 5; matrix products, arithmetic and copies ran while one was open for 44% -> 5% of each run, Pallas kernels for 0% -> 0%
where the time goes in v1:
time: 297 us; the launch traced here: 293 us
  waiting for transfers between devices  127 us (43%)
  matrix products  70.8 us (24%)
  other arithmetic  36.9 us (12%)
  starting transfers between devices  24 us (8%)
  local copies, waits for them, and re-layouts  17.3 us (6%)
  between operations  15.2 us (5%)
    all_gather x1, waiting for transfers between devices, in_one_piece(): lax.all_gather(both, axis, axis=dim, tiled=True)  56.6 us
    all_to_all x1, waiting for transfers between devices, extend_waves(): lax.all_to_all(jnp.stack(lax.axis_size(lane_axis) * [message]), axis_name...  37 us
    dot_general x16, matrix products, attend(): jnp.einsum('qhd,khd->hqk', query_heads, paired_piece[0], preferred_elemen...  24.5 us
    all_to_all x2, waiting for transfers between devices, copy_for_each(): lax.all_to_all(jnp.broadcast_to(value[None], (devices, *value.shape)), ax...  23.4 us
    another operation x20, other arithmetic, block_pass(): jax.scipy.linalg.solve_triangular(weigh_steer + diagonal, entering, lower...  20.1 us
    dot_general x16, matrix products, attend(): jnp.einsum('hqk,khd->qhd', weights.astype(jnp.bfloat16), paired_piece[1],...  14.4 us
    all_to_all x2, starting transfers between devices, copy_for_each(): lax.all_to_all(jnp.broadcast_to(value[None], (devices, *value.shape)), ax...  12.1 us
    all_to_all x1, waiting for transfers between devices, sent_and_summed(): lax.all_to_all(cut_along(value, dim, devices), axis, 0, 0, tiled=True)  9.8 us
  transfers between devices with their start and end apart: 5, of which 5 were waited for; matrix products, arithmetic and copies ran while one was open for 5% of the time, Pallas kernels for 0%

profile of v1, /device:TPU:504, one launch (start us, length us, event | category | flops | bytes accessed | tf_op | source)
XLA Modules:
  0.0 292.7 jit_solution(6616710769927708243)
XLA Ops:
  16.1 4.3 %all-to-all-start = ((bf16[8,128,256]{1,2,0:T(8,128)(2,1)}), bf16[8,128,256]{1,2,0:T(8,128)(2,1)S(1)}, u32[]{:S(2)}, u32[]{:S(2)}) async-start(bf16[8,128,256]{1,2,0:T(8,128)(2,1)} %broadcast_in_dim.72), calls=%async_computation | async-start | bytes 1048576 | tf_op jit(solution)/shard_map/all_to_all | solution.py:29
  22.1 8.6 %all-to-all-done = bf16[8,128,256]{1,2,0:T(8,128)(2,1)S(1)} async-done(((bf16[8,128,256]{1,2,0:T(8,128)(2,1)}), bf16[8,128,256]{1,2,0:T(8,128)(2,1)S(1)}, u32[]{:S(2)}, u32[]{:S(2)}) %all-to-all-start) | async-done | bytes 524320 | tf_op jit(solution)/shard_map/all_to_all | solution.py:29
  33.3 56.6 %all-gather.2.cloned.1.call-done = bf16[2048,1024]{1,0:T(8,128)(2,1)} async-done(((bf16[128,1024]{1,0:T(8,128)(2,1)}), bf16[2048,1024]{1,0:T(8,128)(2,1)}) %all-gather.2.cloned.1.call-update) | async-done | bytes 4194320 | tf_op jit(solution)/shard_map/all_gather | solution.py:51
  94.8 48.1 %while.30 = (s32[]{:T(128)}, f32[2,128,64]{1,2,0:T(8,128)S(1)}, f32[4,32,2,128]{3,1,0,2:T(8,128)S(1)}, f32[4,32,2,64]{3,2,1,0:T(2,128)S(1)}, bf16[4,32,2,64]{3,2...) while((s32[]{:T(128)}, f32[2,128,64]{1,2,0:T(8,128)S(1)}, ...), condition=%wide.region_6.7_spmd, body=%wide.region_2.6_spmd.sunk | while | flops 11161506 | bytes 3108997 | solution.py:252
  95.1 1.8 fusion.243
  99.1 4.9 %custom-call.8 = f32[2,1,32,32]{2,3,1,0:T(8,128)S(1)} custom-call(f32[2,1,32,32]{3,2,1,0:T(8,128)S(1)} %fusion.247), custom_call_target="InvertDiagBlocksLowerTriangular" | custom-call | tf_op jit(solution)/shard_map/while/body/eval_jaxpr/jit(_solve_triangular)/vmap()/triangular_solve | solution.py:142
  107.1 1.8 fusion.243
  111.2 4.9 %custom-call.8 = f32[2,1,32,32]{2,3,1,0:T(8,128)S(1)} custom-call(f32[2,1,32,32]{3,2,1,0:T(8,128)S(1)} %fusion.247), custom_call_target="InvertDiagBlocksLowerTriangular" | custom-call | tf_op jit(solution)/shard_map/while/body/eval_jaxpr/jit(_solve_triangular)/vmap()/triangular_solve | solution.py:142
  119.1 1.8 fusion.243
  123.2 4.9 %custom-call.8 = f32[2,1,32,32]{2,3,1,0:T(8,128)S(1)} custom-call(f32[2,1,32,32]{3,2,1,0:T(8,128)S(1)} %fusion.247), custom_call_target="InvertDiagBlocksLowerTriangular" | custom-call | tf_op jit(solution)/shard_map/while/body/eval_jaxpr/jit(_solve_triangular)/vmap()/triangular_solve | solution.py:142
  131.2 1.8 fusion.243
  135.2 4.9 %custom-call.8 = f32[2,1,32,32]{2,3,1,0:T(8,128)S(1)} custom-call(f32[2,1,32,32]{3,2,1,0:T(8,128)S(1)} %fusion.247), custom_call_target="InvertDiagBlocksLowerTriangular" | custom-call | tf_op jit(solution)/shard_map/while/body/eval_jaxpr/jit(_solve_triangular)/vmap()/triangular_solve | solution.py:142
  144.1 7.8 %all-to-all-start.1 = ((bf16[16,256,64]{1,2,0:T(8,128)(2,1)}), bf16[16,256,64]{1,2,0:T(8,128)(2,1)S(1)}, u32[]{:S(2)}, u32[]{:S(2)}) async-start(bf16[16,256,64]{1,2,0:T(8,128)(2,1)} %broadcast_in_dim.104), calls=%async_computation.1 | async-start | bytes 1048576 | tf_op jit(solution)/shard_map/all_to_all | solution.py:29
  156.8 14.8 %all-to-all-done.1 = bf16[16,256,64]{1,2,0:T(8,128)(2,1)S(1)} async-done(((bf16[16,256,64]{1,2,0:T(8,128)(2,1)}), bf16[16,256,64]{1,2,0:T(8,128)(2,1)S(1)}, u32[]{:S(2)}, u32[]{:S(2)}) %all-to-all-start.1) | async-done | bytes 524320 | tf_op jit(solution)/shard_map/all_to_all | solution.py:29
  172.8 6.0 %all-to-all-start.2 = ((bf16[16,1,2,128,1,128]{5,3,2,4,1,0:T(8,128)(2,1)}), bf16[16,1,2,128,1,128]{5,3,2,4,1,0:T(8,128)(2,1)}, u32[]{:S(2)}, u32[]{:S(2)}) async-start(bf16[16,1,2,128,1,128]{5,3,2,4,1,0:T(8,128)(2,1)} %stack.10), calls=%async_computation.2 | async-start | bytes 2097152 | tf_op jit(solution)/shard_map/all_to_all | solution.py:13
  182.8 1.7 fusion.133
  184.5 37.0 %all-to-all-done.2 = bf16[16,1,2,128,1,128]{5,3,2,4,1,0:T(8,128)(2,1)} async-done(((bf16[16,1,2,128,1,128]{5,3,2,4,1,0:T(8,128)(2,1)}), bf16[16,1,2,128,1,128]{5,3,2,4,1,0:T(8,128)(2,1)}, u32[]{:S(2)}, u32[]{:S(2)}) %all-to-all-start.2) | async-done | bytes 1048608 | tf_op jit(solution)/shard_map/all_to_all | solution.py:13
  221.5 45.0 %while.31 = (s32[]{:T(128)}, f32[128,1,128]{0,2,1:T(8,128)S(1)}, f32[1,128]{1,0:T(1,128)S(1)}, f32[1,128]{1,0:T(1,128)S(1)}, s32[]{:T(128)}, /*index=5*/bf16[16,...) while((s32[]{:T(128)}, f32[128,1,128]{0,2,1:T(8,128)S(1)}, ...), condition=%wide.region_18.19_spmd.clone, body=%wide.region_12.18_spmd.clone.sunk | while | flops 11075848 | bytes 960331 | solution.py:319
  221.5 2.9 conditional.3
  224.4 3.0 %conditional.3 = ((f32[128,1,128]{0,2,1:T(8,128)S(1)}, f32[1,128]{1,0:T(1,128)S(1)}, f32[1,128]{1,0:T(1,128)S(1)})) conditional(s32[]{:T(128)} %convert_element_type.212, (f32[128,1,128]{0,2,1:T(8,128)S(1)}, f32[1,128]{1,0:T(1,128)S(1)}, f32[1,128]{1,0:T(1,128)S(1)}) %tuple.100, (s32[]{:T(128)}, bf16[16,2,128,1,128]{4,2,3,1,0:T(8,128)(2,1)}, ...), branch_computations={%region_13.13_spmd, %region_14.17_spmd} | conditional | flops 11075843 | bytes 959580 | solution.py:315
  224.5 1.6 fusion.69
  227.4 3.0 %conditional.3 = ((f32[128,1,128]{0,2,1:T(8,128)S(1)}, f32[1,128]{1,0:T(1,128)S(1)}, f32[1,128]{1,0:T(1,128)S(1)})) conditional(s32[]{:T(128)} %convert_element_type.212, (f32[128,1,128]{0,2,1:T(8,128)S(1)}, f32[1,128]{1,0:T(1,128)S(1)}, f32[1,128]{1,0:T(1,128)S(1)}) %tuple.100, (s32[]{:T(128)}, bf16[16,2,128,1,128]{4,2,3,1,0:T(8,128)(2,1)}, ...), branch_computations={%region_13.13_spmd, %region_14.17_spmd} | conditional | flops 11075843 | bytes 959580 | solution.py:315
  227.5 1.6 fusion.69
  230.5 3.0 %conditional.3 = ((f32[128,1,128]{0,2,1:T(8,128)S(1)}, f32[1,128]{1,0:T(1,128)S(1)}, f32[1,128]{1,0:T(1,128)S(1)})) conditional(s32[]{:T(128)} %convert_element_type.212, (f32[128,1,128]{0,2,1:T(8,128)S(1)}, f32[1,128]{1,0:T(1,128)S(1)}, f32[1,128]{1,0:T(1,128)S(1)}) %tuple.100, (s32[]{:T(128)}, bf16[16,2,128,1,128]{4,2,3,1,0:T(8,128)(2,1)}, ...), branch_computations={%region_13.13_spmd, %region_14.17_spmd} | conditional | flops 11075843 | bytes 959580 | solution.py:315
  230.5 1.6 fusion.69
  233.5 3.0 %conditional.3 = ((f32[128,1,128]{0,2,1:T(8,128)S(1)}, f32[1,128]{1,0:T(1,128)S(1)}, f32[1,128]{1,0:T(1,128)S(1)})) conditional(s32[]{:T(128)} %convert_element_type.212, (f32[128,1,128]{0,2,1:T(8,128)S(1)}, f32[1,128]{1,0:T(1,128)S(1)}, f32[1,128]{1,0:T(1,128)S(1)}) %tuple.100, (s32[]{:T(128)}, bf16[16,2,128,1,128]{4,2,3,1,0:T(8,128)(2,1)}, ...), branch_computations={%region_13.13_spmd, %region_14.17_spmd} | conditional | flops 11075843 | bytes 959580 | solution.py:315
  233.5 1.6 fusion.69
  236.5 3.0 %conditional.3 = ((f32[128,1,128]{0,2,1:T(8,128)S(1)}, f32[1,128]{1,0:T(1,128)S(1)}, f32[1,128]{1,0:T(1,128)S(1)})) conditional(s32[]{:T(128)} %convert_element_type.212, (f32[128,1,128]{0,2,1:T(8,128)S(1)}, f32[1,128]{1,0:T(1,128)S(1)}, f32[1,128]{1,0:T(1,128)S(1)}) %tuple.100, (s32[]{:T(128)}, bf16[16,2,128,1,128]{4,2,3,1,0:T(8,128)(2,1)}, ...), branch_computations={%region_13.13_spmd, %region_14.17_spmd} | conditional | flops 11075843 | bytes 959580 | solution.py:315
  236.5 1.6 fusion.69
  239.5 3.0 %conditional.3 = ((f32[128,1,128]{0,2,1:T(8,128)S(1)}, f32[1,128]{1,0:T(1,128)S(1)}, f32[1,128]{1,0:T(1,128)S(1)})) conditional(s32[]{:T(128)} %convert_element_type.212, (f32[128,1,128]{0,2,1:T(8,128)S(1)}, f32[1,128]{1,0:T(1,128)S(1)}, f32[1,128]{1,0:T(1,128)S(1)}) %tuple.100, (s32[]{:T(128)}, bf16[16,2,128,1,128]{4,2,3,1,0:T(8,128)(2,1)}, ...), branch_computations={%region_13.13_spmd, %region_14.17_spmd} | conditional | flops 11075843 | bytes 959580 | solution.py:315
  239.5 1.6 fusion.69
  242.5 3.0 %conditional.3 = ((f32[128,1,128]{0,2,1:T(8,128)S(1)}, f32[1,128]{1,0:T(1,128)S(1)}, f32[1,128]{1,0:T(1,128)S(1)})) conditional(s32[]{:T(128)} %convert_element_type.212, (f32[128,1,128]{0,2,1:T(8,128)S(1)}, f32[1,128]{1,0:T(1,128)S(1)}, f32[1,128]{1,0:T(1,128)S(1)}) %tuple.100, (s32[]{:T(128)}, bf16[16,2,128,1,128]{4,2,3,1,0:T(8,128)(2,1)}, ...), branch_computations={%region_13.13_spmd, %region_14.17_spmd} | conditional | flops 11075843 | bytes 959580 | solution.py:315
  242.5 1.6 fusion.69
  245.5 3.0 %conditional.3 = ((f32[128,1,128]{0,2,1:T(8,128)S(1)}, f32[1,128]{1,0:T(1,128)S(1)}, f32[1,128]{1,0:T(1,128)S(1)})) conditional(s32[]{:T(128)} %convert_element_type.212, (f32[128,1,128]{0,2,1:T(8,128)S(1)}, f32[1,128]{1,0:T(1,128)S(1)}, f32[1,128]{1,0:T(1,128)S(1)}) %tuple.100, (s32[]{:T(128)}, bf16[16,2,128,1,128]{4,2,3,1,0:T(8,128)(2,1)}, ...), branch_computations={%region_13.13_spmd, %region_14.17_spmd} | conditional | flops 11075843 | bytes 959580 | solution.py:315
  245.5 1.6 fusion.69
  248.5 3.0 %conditional.3 = ((f32[128,1,128]{0,2,1:T(8,128)S(1)}, f32[1,128]{1,0:T(1,128)S(1)}, f32[1,128]{1,0:T(1,128)S(1)})) conditional(s32[]{:T(128)} %convert_element_type.212, (f32[128,1,128]{0,2,1:T(8,128)S(1)}, f32[1,128]{1,0:T(1,128)S(1)}, f32[1,128]{1,0:T(1,128)S(1)}) %tuple.100, (s32[]{:T(128)}, bf16[16,2,128,1,128]{4,2,3,1,0:T(8,128)(2,1)}, ...), branch_computations={%region_13.13_spmd, %region_14.17_spmd} | conditional | flops 11075843 | bytes 959580 | solution.py:315
  248.5 1.6 fusion.69
  251.5 3.0 %conditional.3 = ((f32[128,1,128]{0,2,1:T(8,128)S(1)}, f32[1,128]{1,0:T(1,128)S(1)}, f32[1,128]{1,0:T(1,128)S(1)})) conditional(s32[]{:T(128)} %convert_element_type.212, (f32[128,1,128]{0,2,1:T(8,128)S(1)}, f32[1,128]{1,0:T(1,128)S(1)}, f32[1,128]{1,0:T(1,128)S(1)}) %tuple.100, (s32[]{:T(128)}, bf16[16,2,128,1,128]{4,2,3,1,0:T(8,128)(2,1)}, ...), branch_computations={%region_13.13_spmd, %region_14.17_spmd} | conditional | flops 11075843 | bytes 959580 | solution.py:315
  251.5 1.6 fusion.69
  254.5 3.0 %conditional.3 = ((f32[128,1,128]{0,2,1:T(8,128)S(1)}, f32[1,128]{1,0:T(1,128)S(1)}, f32[1,128]{1,0:T(1,128)S(1)})) conditional(s32[]{:T(128)} %convert_element_type.212, (f32[128,1,128]{0,2,1:T(8,128)S(1)}, f32[1,128]{1,0:T(1,128)S(1)}, f32[1,128]{1,0:T(1,128)S(1)}) %tuple.100, (s32[]{:T(128)}, bf16[16,2,128,1,128]{4,2,3,1,0:T(8,128)(2,1)}, ...), branch_computations={%region_13.13_spmd, %region_14.17_spmd} | conditional | flops 11075843 | bytes 959580 | solution.py:315
  254.5 1.6 fusion.69
  257.5 3.0 %conditional.3 = ((f32[128,1,128]{0,2,1:T(8,128)S(1)}, f32[1,128]{1,0:T(1,128)S(1)}, f32[1,128]{1,0:T(1,128)S(1)})) conditional(s32[]{:T(128)} %convert_element_type.212, (f32[128,1,128]{0,2,1:T(8,128)S(1)}, f32[1,128]{1,0:T(1,128)S(1)}, f32[1,128]{1,0:T(1,128)S(1)}) %tuple.100, (s32[]{:T(128)}, bf16[16,2,128,1,128]{4,2,3,1,0:T(8,128)(2,1)}, ...), branch_computations={%region_13.13_spmd, %region_14.17_spmd} | conditional | flops 11075843 | bytes 959580 | solution.py:315
  260.5 3.0 %conditional.3 = ((f32[128,1,128]{0,2,1:T(8,128)S(1)}, f32[1,128]{1,0:T(1,128)S(1)}, f32[1,128]{1,0:T(1,128)S(1)})) conditional(s32[]{:T(128)} %convert_element_type.212, (f32[128,1,128]{0,2,1:T(8,128)S(1)}, f32[1,128]{1,0:T(1,128)S(1)}, f32[1,128]{1,0:T(1,128)S(1)}) %tuple.100, (s32[]{:T(128)}, bf16[16,2,128,1,128]{4,2,3,1,0:T(8,128)(2,1)}, ...), branch_computations={%region_13.13_spmd, %region_14.17_spmd} | conditional | flops 11075843 | bytes 959580 | solution.py:315
  260.5 1.6 fusion.69
  263.5 3.0 %conditional.3 = ((f32[128,1,128]{0,2,1:T(8,128)S(1)}, f32[1,128]{1,0:T(1,128)S(1)}, f32[1,128]{1,0:T(1,128)S(1)})) conditional(s32[]{:T(128)} %convert_element_type.212, (f32[128,1,128]{0,2,1:T(8,128)S(1)}, f32[1,128]{1,0:T(1,128)S(1)}, f32[1,128]{1,0:T(1,128)S(1)}) %tuple.100, (s32[]{:T(128)}, bf16[16,2,128,1,128]{4,2,3,1,0:T(8,128)(2,1)}, ...), branch_computations={%region_13.13_spmd, %region_14.17_spmd} | conditional | flops 11075843 | bytes 959580 | solution.py:315
  266.6 2.4 fusion.70
  269.0 5.8 %all-to-all-start.3 = ((bf16[8,16,2048]{2,1,0:T(8,128)(2,1)}), bf16[8,16,2048]{2,1,0:T(8,128)(2,1)S(1)}, u32[]{:S(2)}, u32[]{:S(2)}) async-start(bf16[8,16,2048]{2,1,0:T(8,128)(2,1)} %bitcast.67), calls=%async_computation.3 | async-start | bytes 1048576 | tf_op jit(solution)/shard_map/all_to_all | solution.py:105
  275.4 9.8 %all-to-all-done.3 = bf16[8,16,2048]{2,1,0:T(8,128)(2,1)S(1)} async-done(((bf16[8,16,2048]{2,1,0:T(8,128)(2,1)}), bf16[8,16,2048]{2,1,0:T(8,128)(2,1)S(1)}, u32[]{:S(2)}, u32[]{:S(2)}) %all-to-all-start.3) | async-done | bytes 524320 | tf_op jit(solution)/shard_map/all_to_all | solution.py:105
  (365 shorter events, 74.6 us)
Async XLA Ops:
  7.2 175.6 %copy-start = (bf16[128,2048]{1,0:T(8,128)(2,1)S(1)}, bf16[128,2048]{1,0:T(8,128)(2,1)}, u32[]{:S(2)}) copy-start(bf16[128,2048]{1,0:T(8,128)(2,1)} %param.48) | copy-start | bytes 1572868
  7.2 24.9 %copy-start.3 = (bf16[2048,64]{0,1:T(8,128)(2,1)S(1)}, bf16[2048,64]{0,1:T(8,128)(2,1)}, u32[]{:S(2)}) copy-start(bf16[2048,64]{0,1:T(8,128)(2,1)} %param.34) | copy-start | bytes 786436
  7.2 24.9 %copy-start.5 = (bf16[64,128]{1,0:T(8,128)(2,1)S(1)}, bf16[64,128]{1,0:T(8,128)(2,1)}, u32[]{:S(2)}) copy-start(bf16[64,128]{1,0:T(8,128)(2,1)} %param.35) | copy-start | bytes 49156
  7.2 24.9 %copy-start.7 = (f32[128]{0:T(128)S(1)}, f32[128]{0:T(128)}, u32[]{:S(2)}) copy-start(f32[128]{0:T(128)} %param.38) | copy-start | bytes 1540
  7.2 25.5 %copy-start.4 = (bf16[2048,64]{0,1:T(8,128)(2,1)S(1)}, bf16[2048,64]{0,1:T(8,128)(2,1)}, u32[]{:S(2)}) copy-start(bf16[2048,64]{0,1:T(8,128)(2,1)} %param.36) | copy-start | bytes 786436
  7.2 25.5 %copy-start.6 = (bf16[64,128]{1,0:T(8,128)(2,1)S(1)}, bf16[64,128]{1,0:T(8,128)(2,1)}, u32[]{:S(2)}) copy-start(bf16[64,128]{1,0:T(8,128)(2,1)} %param.37) | copy-start | bytes 49156
  7.2 25.5 %copy-start.8 = (f32[128]{0:T(128)S(1)}, f32[128]{0:T(128)}, u32[]{:S(2)}) copy-start(f32[128]{0:T(128)} %param.39) | copy-start | bytes 1540
  7.2 82.6 %all-gather.2.cloned.1.call-start = ((), (), s32[]{:S(2)}) async-start(), calls=%async_computation.4 | async-start | bytes 4456448 | tf_op jit(solution)/shard_map/all_gather | solution.py:51
  13.5 0.7 copy-start.2
  16.1 14.6 %all-to-all-start = ((bf16[8,128,256]{1,2,0:T(8,128)(2,1)}), bf16[8,128,256]{1,2,0:T(8,128)(2,1)S(1)}, u32[]{:S(2)}, u32[]{:S(2)}) async-start(bf16[8,128,256]{1,2,0:T(8,128)(2,1)} %broadcast_in_dim.72), calls=%async_computation | async-start | bytes 1048576 | tf_op jit(solution)/shard_map/all_to_all | solution.py:29
  144.1 27.4 %all-to-all-start.1 = ((bf16[16,256,64]{1,2,0:T(8,128)(2,1)}), bf16[16,256,64]{1,2,0:T(8,128)(2,1)S(1)}, u32[]{:S(2)}, u32[]{:S(2)}) async-start(bf16[16,256,64]{1,2,0:T(8,128)(2,1)} %broadcast_in_dim.104), calls=%async_computation.1 | async-start | bytes 1048576 | tf_op jit(solution)/shard_map/all_to_all | solution.py:29
  172.8 48.7 %all-to-all-start.2 = ((bf16[16,1,2,128,1,128]{5,3,2,4,1,0:T(8,128)(2,1)}), bf16[16,1,2,128,1,128]{5,3,2,4,1,0:T(8,128)(2,1)}, u32[]{:S(2)}, u32[]{:S(2)}) async-start(bf16[16,1,2,128,1,128]{5,3,2,4,1,0:T(8,128)(2,1)} %stack.10), calls=%async_computation.2 | async-start | bytes 2097152 | tf_op jit(solution)/shard_map/all_to_all | solution.py:13
  180.7 2.1 copy-start.9
  182.8 83.8 %copy-start.1 = (bf16[128,2048]{1,0:T(8,128)(2,1)S(1)}, bf16[128,2048]{1,0:T(8,128)(2,1)}, u32[]{:S(2)}) copy-start(bf16[128,2048]{1,0:T(8,128)(2,1)} %param.49) | copy-start | bytes 1572868
  269.0 16.1 %all-to-all-start.3 = ((bf16[8,16,2048]{2,1,0:T(8,128)(2,1)}), bf16[8,16,2048]{2,1,0:T(8,128)(2,1)S(1)}, u32[]{:S(2)}, u32[]{:S(2)}) async-start(bf16[8,16,2048]{2,1,0:T(8,128)(2,1)} %bitcast.67), calls=%async_computation.3 | async-start | bytes 1048576 | tf_op jit(solution)/shard_map/all_to_all | solution.py:105
Sparse Core Ops, SparseCore 0:
  14.4 75.4 all-gather.1
